TPU v7x, 32 devices: a whole 2x2x4 slice. The times are simulated.
32 devices in a mesh: sp: 16 (over z, y, x), tp: 2 (over core).
Axes of the slice: x: 2, y: 2, z: 4, core: 2. Of those that a mesh axis runs over, the one named last changes fastest.
Arguments:
- ssm_input: bfloat16 [4096, 1024], P('sp', 'tp'), may hold values from -6 to 6
- lam_real: float32 [64, 64], P('tp'), may hold values from -0.034 to -2.197265625e-05, as said below
- lam_imag: float32 [64, 64], P('tp'), may hold values from -3 to 3, as said below
- state_in: float32 [2, 64, 16, 64], P(None, 'tp'), may hold values from -2 to 2
- read_out: float32 [64, 128, 16], P('tp'), may hold values from -0.5 to 0.5
- channel_skip: float32 [1024], P('tp'), may hold values from -3 to 3
- glu_weight: bfloat16 [1024, 1024], replicated, may hold values from -0.1875 to 0.1875
- out_weight: bfloat16 [1024, 2048], replicated, may hold values from -0.375 to 0.375
- residual: bfloat16 [4096, 2048], P(('sp', 'tp')), may hold values from -6 to 6
- norm_gain: float32 [2048], replicated, may hold values from 0.1 to 1.9
- expert_ids: int32 [4096, 2], P(('sp', 'tp')), may hold values from 0 to 31, as said below
- route_weight: float32 [4096, 2], P(('sp', 'tp')), may hold values from 0.25 to 1
- expert_gate: bfloat16 [32, 2048, 512], P(('sp', 'tp')), may hold values from -0.125 to 0.125
- expert_up: bfloat16 [32, 2048, 512], P(('sp', 'tp')), may hold values from -0.125 to 0.125
- expert_down: bfloat16 [32, 512, 2048], P(('sp', 'tp')), may hold values from -0.25 to 0.25
Outputs:
- layer_out: bfloat16 [4096, 2048], P(('sp', 'tp'))
Inputs may be any that keep to these rules, and one draw needn't show every extreme that they name: `lam_real`: strictly negative. `lam_imag`: magnitude at least 0.5. `expert_ids`: A token's two experts differ and lie in the same group of 8 consecutive experts. Among the 128 rows of one device (aligned blocks) no expert is named more than 16 times, and some expert exactly 16 times; every expert is named in every such block.
All inputs are finite; a program needn't handle non-finite values.
Results may differ from a plain program's by a relative error of at most 0.006.
Values may be sent and summed in bfloat16 or wider, within the bound.
A program may use at most 128 MiB of HBM per device.

v0:
```python
import jax
import jax.numpy as jnp
from jax import lax
from jax.sharding import PartitionSpec as P

GROUPS = 4


EPSILON = 1e-06


def prefix(value, axis, join, neutral):
    count, mine = (lax.axis_size(axis), lax.axis_index(axis))
    pieces = jax.tree.map(lambda part: lax.all_gather(part, axis), value)
    so_far = jax.tree.map(
        lambda part, zero: jnp.full_like(part, 0) + jnp.asarray(zero, part.dtype), value, neutral
    )

    def hop(position, so_far):
        longer = join(so_far, jax.tree.map(lambda part: part[position], pieces))
        return jax.tree.map(lambda new, old: jnp.where(position < mine, new, old), longer, so_far)

    return lax.fori_loop(0, count - 1, hop, so_far)


def discretize(lam_real, lam_imag, state_in):
    magnitude = jnp.exp(lam_real)
    decay_re = magnitude * jnp.cos(lam_imag)
    decay_im = magnitude * jnp.sin(lam_imag)
    numer_re = decay_re - 1.0
    denom = lam_real * lam_real + lam_imag * lam_imag
    hold_re = ((numer_re * lam_real + decay_im * lam_imag) / denom)[:, None, :]
    hold_im = ((decay_im * lam_real - numer_re * lam_imag) / denom)[:, None, :]
    drive_re = hold_re * state_in[0] - hold_im * state_in[1]
    drive_im = hold_re * state_in[1] + hold_im * state_in[0]
    drive = jnp.concatenate([drive_re, drive_im], axis=-1).astype(jnp.bfloat16)
    return (decay_re, decay_im, drive)


def powers(lam_real, lam_imag, exponent):
    magnitude = jnp.exp(exponent[:, None, None] * lam_real[None])
    angle = exponent[:, None, None] * lam_imag[None]
    return (magnitude * jnp.cos(angle), magnitude * jnp.sin(angle))


def combine_steps(earlier, later):
    return (
        later[0] * earlier[0] - later[1] * earlier[1],
        later[0] * earlier[1] + later[1] * earlier[0],
        later[0] * earlier[2] - later[1] * earlier[3] + later[2],
        later[0] * earlier[3] + later[1] * earlier[2] + later[3],
    )


def block_states(push_re, push_im, decay_re, decay_im):
    shape_in = push_re.shape
    flat_re = push_re.reshape(shape_in[0], -1)
    flat_im = push_im.reshape(shape_in[0], -1)
    scale_re = jnp.broadcast_to(decay_re.reshape(1, -1), flat_re.shape)
    scale_im = jnp.broadcast_to(decay_im.reshape(1, -1), flat_im.shape)
    result = lax.associative_scan(combine_steps, (scale_re, scale_im, flat_re, flat_im), axis=0)
    return (result[2].reshape(shape_in), result[3].reshape(shape_in))


def readout(part_re, part_im, read_out):
    stacked = jnp.concatenate([part_re, part_im], axis=-1)
    return jnp.einsum("tgq,gqm->tgm", stacked, read_out, precision=lax.Precision.HIGHEST)


def run_expert(arrived, expert_gate, expert_up, expert_down):
    shape_in = arrived.shape
    flat_rows = arrived.reshape(-1, shape_in[-1])
    gate_part = jnp.dot(flat_rows, expert_gate[0], preferred_element_type=jnp.float32)
    up_part = jnp.dot(flat_rows, expert_up[0], preferred_element_type=jnp.float32)
    hidden = (jax.nn.silu(gate_part) * up_part).astype(jnp.bfloat16)
    answer = jnp.dot(hidden, expert_down[0], preferred_element_type=jnp.float32).astype(
        jnp.bfloat16
    )
    return answer.reshape(shape_in)


def on_device(
    ssm_input,
    lam_real,
    lam_imag,
    state_in,
    read_out,
    channel_skip,
    glu_weight,
    out_weight,
    residual,
    norm_gain,
    expert_ids,
    route_weight,
    expert_gate,
    expert_up,
    expert_down,
):
    token_rows = ssm_input.shape[0]
    group_count = lam_real.shape[0]
    state_size = lam_real.shape[1]
    channels = state_in.shape[2]
    decay_re, decay_im, drive = discretize(lam_real, lam_imag, state_in)
    inputs = ssm_input.reshape(token_rows, group_count, channels)
    pushed = jnp.einsum("tgm,gmp->tgp", inputs, drive, preferred_element_type=jnp.float32)
    push_re = pushed[..., :state_size]
    push_im = pushed[..., state_size:]
    span_re, span_im = powers(lam_real, lam_imag, jnp.full((1,), token_rows, jnp.float32))
    state_re, state_im = block_states(push_re, push_im, decay_re, decay_im)
    final_re = state_re[-1]
    final_im = state_im[-1]
    zeros_state = jnp.zeros_like(final_re)
    identity = (jnp.ones_like(final_re), zeros_state, zeros_state, zeros_state)
    incoming = prefix((span_re[0], span_im[0], final_re, final_im), "sp", combine_steps, identity)
    in_re = incoming[2]
    in_im = incoming[3]
    ahead_re, ahead_im = powers(
        lam_real, lam_imag, jnp.arange(1, token_rows + 1).astype(jnp.float32)
    )
    carried_re = ahead_re * in_re - ahead_im * in_im
    carried_im = ahead_re * in_im + ahead_im * in_re
    read = readout(state_re, state_im, read_out) + readout(carried_re, carried_im, read_out)
    skips = channel_skip.reshape(group_count, channels)
    pre = jax.nn.gelu(read + skips * inputs.astype(jnp.float32)).astype(jnp.bfloat16)
    pre = pre.reshape(token_rows, group_count * channels)
    own_tokens = lax.all_to_all(pre, "tp", split_axis=0, concat_axis=1, tiled=True)
    gate_lin = jnp.dot(own_tokens, glu_weight, preferred_element_type=jnp.float32)
    gated = (own_tokens.astype(jnp.float32) * jax.nn.sigmoid(gate_lin)).astype(jnp.bfloat16)
    mixed = residual.astype(jnp.float32) + jnp.dot(
        gated, out_weight, preferred_element_type=jnp.float32
    )
    normed = (
        mixed * lax.rsqrt(jnp.mean(mixed * mixed, axis=-1, keepdims=True) + EPSILON) * norm_gain
    ).astype(jnp.bfloat16)
    token_count = normed.shape[0]
    model_width = normed.shape[1]
    route_count = expert_ids.shape[1]
    sp_count = lax.axis_size("sp")
    tp_count = lax.axis_size("tp")
    expert_count = sp_count * tp_count
    capacity = token_count * GROUPS // expert_count
    flat_ids = expert_ids.reshape(-1)
    onehot = (flat_ids[:, None] == jnp.arange(expert_count, dtype=jnp.int32)[None, :]).astype(
        jnp.int32
    )
    rank = jnp.sum(jnp.cumsum(onehot, axis=0) * onehot, axis=1) - 1
    position = flat_ids * capacity + rank
    slot_total = expert_count * capacity
    token_of = (
        jnp.zeros((slot_total,), jnp.int32)
        .at[position]
        .set(jnp.arange(token_count * route_count, dtype=jnp.int32) // route_count)
    )
    filled = jnp.zeros((slot_total,), jnp.bool_).at[position].set(True)
    outgoing = jnp.where(filled[:, None], normed[token_of], jnp.zeros((), jnp.bfloat16)).reshape(
        expert_count, capacity, model_width
    )
    answered = run_expert(
        lax.all_to_all(outgoing, ("sp", "tp"), split_axis=0, concat_axis=0, tiled=True),
        expert_gate,
        expert_up,
        expert_down,
    )
    returned = lax.all_to_all(answered, ("sp", "tp"), split_axis=0, concat_axis=0, tiled=True)
    answers = returned.reshape(slot_total, model_width)[position].astype(jnp.float32)
    answers = answers.reshape(token_count, route_count, model_width)
    routed = jnp.sum(answers * route_weight[:, :, None], axis=1)
    return (mixed + routed).astype(jnp.bfloat16)


def solution(mesh):
    placed = (
        P("sp", "tp"),
        P("tp", None),
        P("tp", None),
        P(None, "tp", None, None),
        P("tp", None, None),
        P("tp"),
        P(),
        P(),
        P(("sp", "tp"), None),
        P(),
        P(("sp", "tp"), None),
        P(("sp", "tp"), None),
        P(("sp", "tp"), None, None),
        P(("sp", "tp"), None, None),
        P(("sp", "tp"), None, None),
    )
    return jax.shard_map(
        on_device, mesh=mesh, in_specs=placed, out_specs=P(("sp", "tp"), None), check_vma=False
    )
```

profile of v0, /device:TPU:0, one launch (start us, length us, event | category | flops | bytes accessed | tf_op | source)
XLA Modules:
  0.0 759.2 jit_solution(5685278636584425299)
XLA Ops:
  9.0 39.8 %slice.387 = f32[128,2048]{0,1:T(8,128)} slice(f32[256,2048]{0,1:T(8,128)} %bitcast.121), slice={[1:256:2], [0:2048:1]} | slice | bytes 2097152 | tf_op jit(solution)/shard_map/slice | solution.py:61
  48.8 39.4 %slice.380 = f32[128,2048]{0,1:T(8,128)S(1)} slice(f32[256,2048]{0,1:T(8,128)} %bitcast.122), slice={[0:255:2], [0:2048:1]} | slice | bytes 2097152 | tf_op jit(solution)/shard_map/slice | solution.py:61
  88.2 39.5 %slice.475 = f32[127,2048]{0,1:T(8,128)} slice(f32[256,2048]{0,1:T(8,128)} %bitcast.123), slice={[2:256:2], [0:2048:1]} | slice | bytes 2080768 | tf_op jit(solution)/shard_map/slice | solution.py:61
  127.7 39.8 %slice.381 = f32[128,2048]{0,1:T(8,128)} slice(f32[256,2048]{0,1:T(8,128)} %bitcast.118), slice={[1:256:2], [0:2048:1]} | slice | bytes 2097152 | tf_op jit(solution)/shard_map/slice | solution.py:61
  167.4 40.0 %slice.377 = f32[128,2048]{0,1:T(8,128)} slice(f32[256,2048]{0,1:T(8,128)} %bitcast.119), slice={[0:255:2], [0:2048:1]} | slice | bytes 2097152 | tf_op jit(solution)/shard_map/slice | solution.py:61
  207.5 39.5 %slice.472 = f32[127,2048]{0,1:T(8,128)} slice(f32[256,2048]{0,1:T(8,128)} %bitcast.120), slice={[2:256:2], [0:2048:1]} | slice | bytes 2080768 | tf_op jit(solution)/shard_map/slice | solution.py:61
  330.7 13.5 %pad.121 = f32[64,2048]{1,0:T(8,128)} pad(f32[32,2048]{1,0:T(8,128)} %add.586, f32[]{:T(128)} %constant.70.clone.1), padding=1_0_1x0_0_0 | pad | bytes 786436 | tf_op jit(solution)/shard_map/pad | solution.py:61
  354.2 4.6 pad.124
  358.8 4.6 pad.123
  363.4 4.7 pad.125
  375.9 8.6 %pad.126 = f32[256,2048]{1,0:T(8,128)} pad(f32[128,2048]{1,0:T(8,128)} %pad_maximum_fusion, f32[]{:T(128)} %constant.70.clone.1), padding=0_1_1x0_0_0 | pad | bytes 3145732 | tf_op jit(solution)/shard_map/pad | solution.py:61
  384.6 4.8 pad.127
  390.3 4.0 add.598
  395.5 8.8 %pad.128 = f32[256,2048]{1,0:T(8,128)} pad(f32[128,2048]{1,0:T(8,128)} %pad_maximum_fusion.1, f32[]{:T(128)} %constant.70.clone.1), padding=0_1_1x0_0_0 | pad | bytes 3145732 | tf_op jit(solution)/shard_map/pad | solution.py:61
  404.3 4.8 pad.129
  410.1 4.0 add.601
  414.1 43.8 %all-gather.1 = f32[512,64]{1,0:T(8,128)S(1)} all-gather(f32[32,64]{1,0:T(8,128)S(1)} %copy-done.45), channel_id=3, replica_groups=mesh['sp'=16,'tp'=2] {'sp'}, dimensions={0}, use_global_device_ids=true | all-gather | bytes 139264 | tf_op jit(solution)/shard_map/all_gather | solution.py:14
  457.9 36.8 %all-gather = f32[512,64]{1,0:T(8,128)S(1)} all-gather(f32[32,64]{1,0:T(8,128)S(1)} %copy-done.44), channel_id=2, replica_groups=mesh['sp'=16,'tp'=2] {'sp'}, dimensions={0}, use_global_device_ids=true | all-gather | bytes 139264 | tf_op jit(solution)/shard_map/all_gather | solution.py:14
  497.7 38.9 %all_gather.14 = f32[16,32,64]{2,1,0:T(8,128)S(1)} all-gather(f32[1,32,64]{2,1,0:T(8,128)S(1)} %slice.477), channel_id=1, replica_groups=mesh['sp'=16,'tp'=2] {'sp'}, dimensions={0}, use_global_device_ids=true | all-gather | bytes 139264 | tf_op jit(solution)/shard_map/all_gather | solution.py:14
  539.6 37.0 %all_gather.15 = f32[16,32,64]{2,1,0:T(8,128)S(1)} all-gather(f32[1,32,64]{2,1,0:T(8,128)S(1)} %slice.479), channel_id=1, replica_groups=mesh['sp'=16,'tp'=2] {'sp'}, dimensions={0}, use_global_device_ids=true | all-gather | bytes 139264 | tf_op jit(solution)/shard_map/all_gather | solution.py:14
  577.3 3.8 copy.70
  581.1 3.9 copy.69
  585.0 6.6 fusion.6
  591.7 16.3 %multiply_subtract_fusion = (f32[256,32,64]{2,0,1:T(8,128)S(1)}, f32[256,32,64]{2,0,1:T(8,128)S(1)}) fusion(f32[32,64]{1,0:T(8,128)S(1)} %get-tuple-element.146, f32[32,64]{1,0:T(8,128)S(1)} %get-tuple-element.145, f32[32,64]{1,0:T(8,128)S(1)} %copy-done.41, f32[32,64]{1,0:T(8,128)S(1)} %copy-done.42, f32[256]{0:T(256)S(1)} %copy-done.65), kind=kLoop, calls=%fused_computation.27 | loop fusion | flops 5242880 | bytes 4228096 | tf_op jit(solution)/shard_map/sub | solution.py:120
  608.0 4.3 fusion.50
  621.4 5.0 multiply_reduce_fusion.1
  633.0 50.8 %all_to_all.29 = bf16[32,16,2048]{2,1,0:T(8,128)(2,1)S(1)} all-to-all(bf16[32,16,2048]{2,1,0:T(8,128)(2,1)S(1)} %broadcast_select_fusion), channel_id=1, replica_groups=mesh['sp'=16,'tp'=2] {'sp','tp'}, dimensions={0} | all-to-all | bytes 4194304 | tf_op jit(solution)/shard_map/all_to_all | solution.py:159
  687.4 6.3 convolution_convert_fusion
  693.7 4.0 all-to-all-start.2
  697.8 48.6 %all-to-all-done.2 = bf16[32,16,2048]{2,1,0:T(8,128)(2,1)} async-done(((bf16[32,16,2048]{2,1,0:T(8,128)(2,1)}), bf16[32,16,2048]{2,1,0:T(8,128)(2,1)}, u32[]{:S(2)}, u32[]{:S(2)}) %all-to-all-start.2) | async-done | bytes 2097184 | tf_op jit(solution)/shard_map/all_to_all | solution.py:164
  746.4 4.2 gather_fusion.1
  753.0 4.9 multiply_reduce_fusion
  (322 shorter events, 142.3 us)
Async XLA Ops:
  0.0 687.4 %copy-start = (bf16[1,512,2048]{2,1,0:T(8,128)(2,1)S(1)}, bf16[1,512,2048]{2,1,0:T(8,128)(2,1)}, u32[]{:S(2)}) copy-start(bf16[1,512,2048]{2,1,0:T(8,128)(2,1)} %param.31) | copy-start | bytes 6291460
  167.4 79.5 %copy-start.47 = (f32[32,64]{1,0:T(8,128)S(1)}, f32[32,64]{1,0:T(8,128)}, u32[]{:S(2)}) copy-start(f32[32,64]{1,0:T(8,128)} %get-tuple-element.247) | copy-start | bytes 24580
  167.4 79.6 %copy-start.46 = (f32[32,64]{1,0:T(8,128)S(1)}, f32[32,64]{1,0:T(8,128)}, u32[]{:S(2)}) copy-start(f32[32,64]{1,0:T(8,128)} %get-tuple-element.248) | copy-start | bytes 24580
  247.0 8.6 %copy-start.29 = (f32[2048]{0:T(1024)}, f32[2048]{0:T(1024)S(1)}, u32[]{:S(2)}) copy-start(f32[2048]{0:T(1024)S(1)} %broadcast_in_dim.23) | copy-start | bytes 24580
  247.1 8.5 %copy-start.31 = (f32[2048]{0:T(1024)}, f32[2048]{0:T(1024)S(1)}, u32[]{:S(2)}) copy-start(f32[2048]{0:T(1024)S(1)} %broadcast_in_dim.22) | copy-start | bytes 24580
  255.6 19.1 %copy-start.33 = (f32[2048]{0:T(1024)}, f32[2048]{0:T(1024)S(1)}, u32[]{:S(2)}) copy-start(f32[2048]{0:T(1024)S(1)} %get-tuple-element.201) | copy-start | bytes 24580
  255.6 19.1 %copy-start.35 = (f32[2048]{0:T(1024)}, f32[2048]{0:T(1024)S(1)}, u32[]{:S(2)}) copy-start(f32[2048]{0:T(1024)S(1)} %get-tuple-element.202) | copy-start | bytes 24580
  255.7 25.4 %copy-start.37 = (f32[2048]{0:T(1024)}, f32[2048]{0:T(1024)S(1)}, u32[]{:S(2)}) copy-start(f32[2048]{0:T(1024)S(1)} %get-tuple-element.199) | copy-start | bytes 24580
  255.7 25.4 %copy-start.38 = (f32[2048]{0:T(1024)}, f32[2048]{0:T(1024)S(1)}, u32[]{:S(2)}) copy-start(f32[2048]{0:T(1024)S(1)} %get-tuple-element.200) | copy-start | bytes 24580
  285.6 28.7 %copy-start.9 = (f32[127,2048]{0,1:T(8,128)S(1)}, f32[127,2048]{0,1:T(8,128)}, u32[]{:S(2)}) copy-start(f32[127,2048]{0,1:T(8,128)} %slice.475) | copy-start | bytes 3121156
  314.3 4.3 copy-start.53
  314.3 4.3 copy-start.54
  314.3 4.3 copy-start.55
  314.3 4.3 copy-start.56
  330.7 17.5 %copy-start.34 = (f32[2048]{0:T(1024)S(1)}, f32[2048]{0:T(1024)}, u32[]{:S(2)}) copy-start(f32[2048]{0:T(1024)} %copy-done.33) | copy-start | bytes 24580
  330.7 17.5 %copy-start.36 = (f32[2048]{0:T(1024)S(1)}, f32[2048]{0:T(1024)}, u32[]{:S(2)}) copy-start(f32[2048]{0:T(1024)} %copy-done.35) | copy-start | bytes 24580
  375.9 8.7 %copy-start.8 = (f32[128,2048]{1,0:T(8,128)S(1)}, f32[128,2048]{1,0:T(8,128)}, u32[]{:S(2)}) copy-start(f32[128,2048]{1,0:T(8,128)} %add.593) | copy-start | bytes 3145732
  390.3 4.1 copy-start.14
  395.5 8.8 %copy-start.7 = (f32[128,2048]{1,0:T(8,128)S(1)}, f32[128,2048]{1,0:T(8,128)}, u32[]{:S(2)}) copy-start(f32[128,2048]{1,0:T(8,128)} %add.596) | copy-start | bytes 3145732
  410.1 4.1 copy-start.45
  410.1 47.8 %copy-start.44 = (f32[32,64]{1,0:T(8,128)S(1)}, f32[32,64]{1,0:T(8,128)}, u32[]{:S(2)}) copy-start(f32[32,64]{1,0:T(8,128)} %get-tuple-element.249) | copy-start | bytes 24580
  536.6 40.0 %copy-start.20 = (f32[32,64]{1,0:T(8,128)S(1)}, f32[32,64]{1,0:T(8,128)}, u32[]{:S(2)}) copy-start(f32[32,64]{1,0:T(8,128)} %custom-call) | copy-start | bytes 24580
  585.0 6.7 copy-start.41
  585.0 6.7 copy-start.42
  585.0 6.7 copy-start.65
  608.0 8.6 %copy-start.62 = (s32[128,2]{0,1:T(2,128)S(1)}, s32[128,2]{0,1:T(2,128)}, u32[]{:S(2)}) copy-start(s32[128,2]{0,1:T(2,128)} %param.27) | copy-start | bytes 3076
  612.3 9.1 %copy-start.67 = (bf16[128,2048]{1,0:T(8,128)(2,1)S(1)}, bf16[128,2048]{1,0:T(8,128)(2,1)}, u32[]{:S(2)}) copy-start(bf16[128,2048]{1,0:T(8,128)(2,1)} %param.25) | copy-start | bytes 1572868
  613.1 8.1 %all-to-all-start = ((bf16[2,128,512]{1,2,0:T(8,128)(2,1)}), bf16[2,128,512]{1,2,0:T(8,128)(2,1)S(1)}, u32[]{:S(2)}, u32[]{:S(2)}) async-start(bf16[2,128,512]{1,2,0:T(8,128)(2,1)} %copy.71), calls=%async_computation | async-start | bytes 524288 | tf_op jit(solution)/shard_map/all_to_all | solution.py:126
  621.4 5.1 copy-start.61
  632.9 52.2 %copy-start.66 = (bf16[1,2048,512]{2,1,0:T(8,128)(2,1)S(1)}, bf16[1,2048,512]{2,1,0:T(8,128)(2,1)}, u32[]{:S(2)}) copy-start(bf16[1,2048,512]{2,1,0:T(8,128)(2,1)} %param.29) | copy-start | bytes 6291460
  693.7 52.7 %all-to-all-start.2 = ((bf16[32,16,2048]{2,1,0:T(8,128)(2,1)}), bf16[32,16,2048]{2,1,0:T(8,128)(2,1)}, u32[]{:S(2)}, u32[]{:S(2)}) async-start(bf16[32,16,2048]{2,1,0:T(8,128)(2,1)} %bitcast.129), calls=%async_computation.2 | async-start | bytes 4194304 | tf_op jit(solution)/shard_map/all_to_all | solution.py:164
  753.0 4.9 copy-start.10
  (38 other events, 110.6 us)
where the time goes:
time: 771 us; the launch traced here: 759 us
  local copies, waits for them, and re-layouts  394 us (51%)
  blocking collectives  207 us (27%)
  other arithmetic  74.7 us (10%)
  waiting for transfers between devices  48.6 us (6%)
  matrix products  25.6 us (3%)
    slice x53, local copies, waits for them, and re-layouts, block_states(): lax.associative_scan(combine_steps, (scale_re, scale_im, flat_re, flat_im...  283 us
    all_gather x4, blocking collectives, prefix(): pieces = jax.tree.map(lambda part: lax.all_gather(part, axis), value)  156 us
    pad x28, local copies, waits for them, and re-layouts, block_states(): lax.associative_scan(combine_steps, (scale_re, scale_im, flat_re, flat_im...  60.8 us
    all_to_all x1, blocking collectives, on_device(): lax.all_to_all(outgoing, ('sp', 'tp'), split_axis=0, concat_axis=0, tiled...  50.8 us
    all_to_all x1, waiting for transfers between devices, on_device(): lax.all_to_all(answered, ('sp', 'tp'), split_axis=0, concat_axis=0, tiled...  48.6 us
    add x17, other arithmetic, block_states(): lax.associative_scan(combine_steps, (scale_re, scale_im, flat_re, flat_im...  19.2 us
    unnamed x145, local copies, waits for them, and re-layouts  17.8 us
    sub x1, other arithmetic, on_device(): carried_re = ahead_re * in_re - ahead_im * in_im  16.3 us
  transfers between devices with their start and end apart: 2, of which 1 were waited for; matrix products, arithmetic and copies ran while one was open for 1% of the time, Pallas kernels for 0%

commit v1 on v0

v1 whole, which is shorter than its diff:
```python
import functools

import jax
import jax.numpy as jnp
from jax import lax
from jax.experimental import pallas as pl
from jax.experimental.pallas import tpu as pltpu
from jax.sharding import PartitionSpec as P

GROUPS = 4
EPSILON = 1e-06
LANES = 128
SEGMENTS = 8


def discretize(lam_real, lam_imag, state_in):
    magnitude = jnp.exp(lam_real)
    decay_re = magnitude * jnp.cos(lam_imag)
    decay_im = magnitude * jnp.sin(lam_imag)
    numer_re = decay_re - 1.0
    denom = lam_real * lam_real + lam_imag * lam_imag
    hold_re = ((numer_re * lam_real + decay_im * lam_imag) / denom)[:, None, :]
    hold_im = ((decay_im * lam_real - numer_re * lam_imag) / denom)[:, None, :]
    drive_re = hold_re * state_in[0] - hold_im * state_in[1]
    drive_im = hold_re * state_in[1] + hold_im * state_in[0]
    return drive_re.astype(jnp.bfloat16), drive_im.astype(jnp.bfloat16)


def powers(lam_real, lam_imag, exponent):
    magnitude = jnp.exp(exponent[:, None, None] * lam_real[None])
    angle = exponent[:, None, None] * lam_imag[None]
    return (magnitude * jnp.cos(angle), magnitude * jnp.sin(angle))


def iota(shape, dim):
    return lax.broadcasted_iota(jnp.int32, shape, dim)


def times(a_re, a_im, b_re, b_im):
    return a_re * b_re - a_im * b_im, a_re * b_im + a_im * b_re


def segment_order(rows, back=False):
    length = rows // SEGMENTS
    ordered, token = iota((rows, rows), 1 if back else 0), iota((rows, rows), 0 if back else 1)
    same = (ordered % SEGMENTS) * length + ordered // SEGMENTS == token
    return same.astype(jnp.float32).astype(jnp.bfloat16)


def spread(block, copies, row_group, column_group):
    rows, width = block.shape
    wide = width * copies
    pick = iota((width, wide), 0) == iota((width, wide), 1) % width
    tiled = jnp.dot(
        block, pick.astype(jnp.float32).astype(jnp.bfloat16), preferred_element_type=jnp.float32
    )
    keep = (iota((rows, wide), 0) // row_group) == (iota((rows, wide), 1) // column_group)
    return jnp.where(keep, tiled, 0.0).astype(jnp.bfloat16)


def ssm_ordered(x_ref):
    rows = x_ref.shape[0]
    return jnp.dot(
        segment_order(rows), x_ref[...], preferred_element_type=jnp.float32
    )


def fill_push(x_tile, drive_re_ref, drive_im_ref, tile, channels, push):
    states = drive_re_ref.shape[1]
    copies = LANES // channels
    width = copies * states
    rows = pl.ds(tile * LANES, LANES)
    for part, ref in enumerate((drive_re_ref, drive_im_ref)):
        block = spread(ref[rows, :], copies, channels, states)
        push[:, part * width : (part + 1) * width] = jnp.dot(
            x_tile, block, preferred_element_type=jnp.float32
        )


def run_scan(push, width, decay_re, decay_im, start_re, start_im, keep):
    shape = (SEGMENTS, width)
    decay_re = jnp.broadcast_to(decay_re, shape)
    decay_im = jnp.broadcast_to(decay_im, shape)

    def step(j, carry):
        rows = pl.ds(pl.multiple_of(j * SEGMENTS, SEGMENTS), SEGMENTS)
        next_re, next_im = times(decay_re, decay_im, *carry)
        next_re = next_re + push[rows, :width]
        next_im = next_im + push[rows, width:]
        if keep:
            push[rows, :width] = next_re
            push[rows, width:] = next_im
        return next_re, next_im

    return lax.fori_loop(0, push.shape[0] // SEGMENTS, step, (start_re, start_im), unroll=4)


def ends_kernel(channels, x_ref, drive_re_ref, drive_im_ref, pow_re_ref, pow_im_ref,
                ends_re_ref, ends_im_ref, final_ref, push):
    ordered = ssm_ordered(x_ref).astype(jnp.bfloat16)
    width = push.shape[1] // 2
    total = pow_re_ref.shape[1]
    for tile in range(total // width):
        lanes = slice(tile * width, (tile + 1) * width)
        fill_push(
            ordered[:, tile * LANES : (tile + 1) * LANES], drive_re_ref, drive_im_ref, tile,
            channels, push,
        )
        zero = jnp.zeros((SEGMENTS, width), jnp.float32)
        end_re, end_im = run_scan(
            push, width, pow_re_ref[0:1, lanes], pow_im_ref[0:1, lanes], zero, zero, False
        )
        ends_re_ref[:, lanes] = end_re
        ends_im_ref[:, lanes] = end_im
        seg_re, seg_im = pow_re_ref[1:2, lanes], pow_im_ref[1:2, lanes]
        sum_re, sum_im = end_re[0:1], end_im[0:1]
        for s in range(1, SEGMENTS):
            sum_re, sum_im = times(seg_re, seg_im, sum_re, sum_im)
            sum_re, sum_im = sum_re + end_re[s : s + 1], sum_im + end_im[s : s + 1]
        final_ref[0:1, lanes] = sum_re
        final_ref[1:2, lanes] = sum_im


def mixer_kernel(channels, x_ref, drive_re_ref, drive_im_ref, pow_re_ref, pow_im_ref,
                 ends_re_ref, ends_im_ref, finals_ref, read_ref, skip_ref, out_ref,
                 push, start, pre):
    mine = lax.axis_index("sp")
    wide = ssm_ordered(x_ref)
    ordered = wide.astype(jnp.bfloat16)
    rows = x_ref.shape[0]
    width = push.shape[1] // 2
    total = pow_re_ref.shape[1]
    states = drive_re_ref.shape[1]
    copies = LANES // channels
    for tile in range(total // width):
        lanes = slice(tile * width, (tile + 1) * width)
        span_re, span_im = pow_re_ref[2:3, lanes], pow_im_ref[2:3, lanes]
        zero = jnp.zeros((1, width), jnp.float32)

        def hop(position, so_far):
            new_re, new_im = times(span_re, span_im, *so_far)
            return (new_re + finals_ref[position, 0:1, lanes],
                    new_im + finals_ref[position, 1:2, lanes])

        in_re, in_im = lax.fori_loop(0, mine, hop, (zero, zero))
        seg_re, seg_im = pow_re_ref[1:2, lanes], pow_im_ref[1:2, lanes]
        for s in range(SEGMENTS):
            start[s : s + 1, :width] = in_re
            start[s : s + 1, width:] = in_im
            in_re, in_im = times(seg_re, seg_im, in_re, in_im)
            in_re = in_re + ends_re_ref[s : s + 1, lanes]
            in_im = in_im + ends_im_ref[s : s + 1, lanes]
        own = slice(tile * LANES, (tile + 1) * LANES)
        fill_push(ordered[:, own], drive_re_ref, drive_im_ref, tile, channels, push)
        run_scan(
            push, width, pow_re_ref[0:1, lanes], pow_im_ref[0:1, lanes], start[:, :width],
            start[:, width:], True,
        )
        read = jnp.zeros((rows, LANES), jnp.float32)
        for part in range(2):
            block = read_ref[tile * copies : (tile + 1) * copies,
                             part * states : (part + 1) * states, :]
            block = block.reshape(width, channels).astype(jnp.bfloat16)
            block = spread(block, copies, states, channels)
            read = read + jnp.dot(
                push[:, part * width : (part + 1) * width].astype(jnp.bfloat16), block,
                preferred_element_type=jnp.float32,
            )
        value = jax.nn.gelu(read + skip_ref[0:1, own] * wide[:, own])
        pre[:, own] = value.astype(jnp.bfloat16)
    out_ref[...] = jnp.dot(
        segment_order(rows, back=True), pre[...], preferred_element_type=jnp.float32
    ).astype(jnp.bfloat16)


def mixer(ssm_input, lam_real, lam_imag, state_in, read_out, channel_skip):
    rows, width_in = ssm_input.shape
    groups, states = lam_real.shape
    channels = state_in.shape[2]
    total = groups * states
    width = (LANES // channels) * states
    drive_re, drive_im = discretize(lam_real, lam_imag, state_in)
    drive_re = drive_re.reshape(width_in, states)
    drive_im = drive_im.reshape(width_in, states)
    steps = jnp.asarray([1.0, rows // SEGMENTS, rows], jnp.float32)
    pow_re, pow_im = powers(lam_real, lam_imag, steps)
    pow_re, pow_im = pow_re.reshape(3, total), pow_im.reshape(3, total)
    f32 = jnp.float32
    ends_re, ends_im, final = pl.pallas_call(
        functools.partial(ends_kernel, channels),
        out_shape=(
            jax.ShapeDtypeStruct((SEGMENTS, total), f32),
            jax.ShapeDtypeStruct((SEGMENTS, total), f32),
            jax.ShapeDtypeStruct((2, total), f32),
        ),
        scratch_shapes=[pltpu.VMEM((rows, 2 * width), f32)],
        name="ends",
    )(ssm_input, drive_re, drive_im, pow_re, pow_im)
    finals = lax.all_gather(final, "sp")
    return pl.pallas_call(
        functools.partial(mixer_kernel, channels),
        out_shape=jax.ShapeDtypeStruct((rows, width_in), jnp.bfloat16),
        scratch_shapes=[
            pltpu.VMEM((rows, 2 * width), f32),
            pltpu.VMEM((SEGMENTS, 2 * width), f32),
            pltpu.VMEM((rows, width_in), jnp.bfloat16),
        ],
        name="mixer",
    )(ssm_input, drive_re, drive_im, pow_re, pow_im, ends_re, ends_im, finals, read_out,
      channel_skip.reshape(1, width_in))


def swap_halves(pre):
    half = pre.shape[0] // 2
    me = lax.axis_index("tp")
    kept = lax.dynamic_slice_in_dim(pre, me * half, half, 0)
    given = lax.dynamic_slice_in_dim(pre, (1 - me) * half, half, 0)
    taken = lax.ppermute(given, "tp", [(0, 1), (1, 0)])
    first = jnp.where(me == 0, kept, taken)
    second = jnp.where(me == 0, taken, kept)
    return jnp.concatenate([first, second], axis=1)


def routes(expert_ids, expert_count, capacity):
    tokens = expert_ids.shape[0]
    experts = jnp.arange(expert_count, dtype=jnp.int32)
    onehot = (expert_ids[:, :, None] == experts[None, None, :]).astype(jnp.float32)
    earlier = (jnp.arange(tokens)[:, None] > jnp.arange(tokens)[None, :]).astype(jnp.bfloat16)
    before = jnp.dot(
        earlier, jnp.sum(onehot, axis=1).astype(jnp.bfloat16), preferred_element_type=jnp.float32
    )
    rank = jnp.sum(before[:, None, :] * onehot, axis=-1).astype(jnp.int32)
    return expert_ids * capacity + rank


def run_expert(rows, expert_gate, expert_up, expert_down):
    gate_part = jnp.dot(rows, expert_gate[0], preferred_element_type=jnp.float32)
    up_part = jnp.dot(rows, expert_up[0], preferred_element_type=jnp.float32)
    hidden = (jax.nn.silu(gate_part) * up_part).astype(jnp.bfloat16)
    return jnp.dot(hidden, expert_down[0], preferred_element_type=jnp.float32).astype(
        jnp.bfloat16
    )


def on_device(
    ssm_input,
    lam_real,
    lam_imag,
    state_in,
    read_out,
    channel_skip,
    glu_weight,
    out_weight,
    residual,
    norm_gain,
    expert_ids,
    route_weight,
    expert_gate,
    expert_up,
    expert_down,
):
    f32, bf16 = jnp.float32, jnp.bfloat16
    pre = mixer(ssm_input, lam_real, lam_imag, state_in, read_out, channel_skip)
    own_tokens = swap_halves(pre)
    gate_lin = jnp.dot(own_tokens, glu_weight, preferred_element_type=f32)
    gated = (own_tokens.astype(f32) * jax.nn.sigmoid(gate_lin)).astype(bf16)
    mixed = residual.astype(f32) + jnp.dot(gated, out_weight, preferred_element_type=f32)
    normed = (
        mixed * lax.rsqrt(jnp.mean(mixed * mixed, axis=-1, keepdims=True) + EPSILON) * norm_gain
    ).astype(bf16)
    tokens, model_width = normed.shape
    expert_count = lax.axis_size("sp") * lax.axis_size("tp")
    capacity = tokens * GROUPS // expert_count
    position = routes(expert_ids, expert_count, capacity)
    slots = jnp.arange(expert_count * capacity, dtype=jnp.int32)
    chosen = position[:, :, None] == slots[None, None, :]
    pick = jnp.any(chosen, axis=1).astype(bf16)
    outgoing = lax.dot_general(
        pick, normed, (((0,), (0,)), ((), ())), preferred_element_type=f32
    ).astype(bf16)
    outgoing = outgoing.reshape(expert_count, capacity, model_width)
    arrived = lax.all_to_all(outgoing, ("sp", "tp"), split_axis=0, concat_axis=0, tiled=True)
    answered = run_expert(
        arrived.reshape(-1, model_width), expert_gate, expert_up, expert_down
    ).reshape(arrived.shape)
    returned = lax.all_to_all(answered, ("sp", "tp"), split_axis=0, concat_axis=0, tiled=True)
    returned = returned.reshape(-1, model_width)
    weights = jnp.sum(jnp.where(chosen, route_weight[:, :, None], 0.0), axis=1)
    coarse = weights.astype(bf16)
    fine = (weights - coarse.astype(f32)).astype(bf16)
    routed = jnp.dot(coarse, returned, preferred_element_type=f32) + jnp.dot(
        fine, returned, preferred_element_type=f32
    )
    return (mixed + routed).astype(bf16)


def solution(mesh):
    placed = (
        P("sp", "tp"),
        P("tp", None),
        P("tp", None),
        P(None, "tp", None, None),
        P("tp", None, None),
        P("tp"),
        P(),
        P(),
        P(("sp", "tp"), None),
        P(),
        P(("sp", "tp"), None),
        P(("sp", "tp"), None),
        P(("sp", "tp"), None, None),
        P(("sp", "tp"), None, None),
        P(("sp", "tp"), None, None),
    )
    return jax.shard_map(
        on_device, mesh=mesh, in_specs=placed, out_specs=P(("sp", "tp"), None), check_vma=False
    )
```

time: 771 us -> 194 us (0.25); the launches traced: 759 us -> 193 us
  local copies, waits for them, and re-layouts: 394 us -> 6.99 us
  blocking collectives: 207 us -> 96.9 us
  other arithmetic: 74.7 us -> 4.49 us
  Pallas kernels: 0 us -> 13.1 us
    slice x57 -> x1, local copies, waits for them, and re-layouts: 285 us -> 1.06 us  [discretize(): drive_re = hold_re * state_in[0] - hold_im * state_in[1]]
    all_gather x4 -> x1, blocking collectives: 156 us -> 46.3 us  [mixer(): finals = lax.all_gather(final, 'sp')]
    pad x28 -> x0, local copies, waits for them, and re-layouts: 60.8 us -> none  [block_states(): lax.associative_scan(combine_steps, (scale_re, scale_im, flat_re, flat_im...]
    add x33 -> x1, other arithmetic: 36.4 us -> 0.01 us  [routes(): return expert_ids * capacity + rank]
    sub x3 -> x0, other arithmetic: 17 us -> none  [the longest x1 16.3 us: on_device(): carried_re = ahead_re * in_re - ahead_im * in_im]
    unnamed x145 -> x15, local copies, waits for them, and re-layouts: 17.8 us -> 3.28 us
    pallas_call x0 -> x2, Pallas kernels: none -> 13.1 us  [the longest x1 8.23 us: mixer(): pl.pallas_call(functools.partial(mixer_kernel, channels), out_shape=jax.S...]
    concatenate x13 -> x0, other arithmetic: 8.14 us -> none  [block_states(): lax.associative_scan(combine_steps, (scale_re, scale_im, flat_re, flat_im...]
  transfers between devices with their start and end apart: 2 -> 2, of which waited for: 1 -> 2; matrix products, arithmetic and copies ran while one was open for 1% -> 0% of each run, Pallas kernels for 0% -> 0%
where the time goes in v1:
time: 194 us; the launch traced here: 193 us
  blocking collectives  96.9 us (50%)
  waiting for transfers between devices  49.5 us (26%)
  matrix products  18.5 us (10%)
  Pallas kernels  13.1 us (7%)
  local copies, waits for them, and re-layouts  6.99 us (4%)
  other arithmetic  4.49 us (2%)
  starting transfers between devices  3.79 us (2%)
    all_to_all x1, blocking collectives, on_device(): lax.all_to_all(outgoing, ('sp', 'tp'), split_axis=0, concat_axis=0, tiled...  50.5 us
    all_to_all x1, waiting for transfers between devices, on_device(): lax.all_to_all(answered, ('sp', 'tp'), split_axis=0, concat_axis=0, tiled...  48.6 us
    all_gather x1, blocking collectives, mixer(): finals = lax.all_gather(final, 'sp')  46.3 us
    pallas_call x1, Pallas kernels, mixer(): pl.pallas_call(functools.partial(mixer_kernel, channels), out_shape=jax.S...  8.23 us
    dot_general x1, matrix products, run_expert(): jnp.dot(hidden, expert_down[0], preferred_element_type=jnp.float32)  6.25 us
    pallas_call x1, Pallas kernels, mixer(): pl.pallas_call(functools.partial(ends_kernel, channels), out_shape=(jax.S...  4.85 us
    dot_general x1, matrix products, on_device(): jnp.dot(gated, out_weight, preferred_element_type=f32)  4.17 us
  transfers between devices with their start and end apart: 2, of which 2 were waited for; matrix products, arithmetic and copies ran while one was open for 0% of the time, Pallas kernels for 0%

profile of v1, /device:TPU:0, one launch (start us, length us, event | category | flops | bytes accessed | tf_op | source)
XLA Modules:
  0.0 193.5 jit_solution(8692952380693709474)
XLA Ops:
  0.0 0.0 copy-start
  0.0 0.9 mul.166
  0.9 0.8 fusion.39
  1.8 0.8 mul.169
  2.6 1.1 fusion.47
  3.6 1.6 fusion.38
  5.2 0.8 fusion.25
  6.0 4.9 %ends.1 = (f32[8,2048]{1,0:T(8,128)}, f32[8,2048]{1,0:T(8,128)}, f32[2,2048]{1,0:T(2,128)}) custom-call(bf16[256,512]{1,0:T(8,128)(2,1)} %x_ref.3, bf16[512,64]{1,0:T(8,128)(2,1)} %get-tuple-element.12.drive_re_ref, bf16[512,64]{1,0:T(8,128)(2,1)} %get-tuple-element.11.drive_im_ref, f32[3,2048]{1,0:T(4,128)} %get-tuple-element.20.pow_re_ref, ...), custom_call_target="tpu_custom_call" | custom-call | tf_op jit(solution)/shard_map/ends/pallas_call | solution.py:189
  10.9 46.3 %all-gather.1.finals_ref = f32[16,2,2048]{2,1,0:T(2,128)} all-gather(f32[1,2,2048]{2,1,0:T(2,128)} %bitcast.57), channel_id=2, replica_groups=mesh['sp'=16,'tp'=2] {'sp'}, dimensions={0}, use_global_device_ids=true | all-gather | bytes 278528 | tf_op jit(solution)/shard_map/all_gather | solution.py:199
  57.2 1.9 %copy.27.read_ref = f32[32,128,16]{2,1,0:T(8,128)} copy(f32[32,128,16]{1,2,0:T(8,128)S(1)} %copy-done.2) | data formatting | bytes 524288 | tf_op args[4]
  59.2 8.2 %mixer.1 = bf16[256,512]{1,0:T(8,128)(2,1)} custom-call(bf16[256,512]{1,0:T(8,128)(2,1)} %x_ref.3, bf16[512,64]{1,0:T(8,128)(2,1)} %get-tuple-element.12.drive_re_ref, bf16[512,64]{1,0:T(8,128)(2,1)} %get-tuple-element.11.drive_im_ref, f32[3,2048]{1,0:T(4,128)} %get-tuple-element.20.pow_re_ref, f32[3,2048]{1,0:T(4,128)} %get-tuple-element.19.pow_im_ref, ...), custom_call_target="tpu_custom_call" | custom-call | tf_op jit(solution)/shard_map/mixer/pallas_call | solution.py:200
  67.4 0.9 constant_dynamic-slice_fusion
  68.3 0.1 collective-permute-start
  68.4 0.0 copy-done.3
  68.4 0.1 fusion.36
  68.6 0.1 fusion.21
  68.8 1.0 collective-permute-done
  69.7 1.0 broadcast_select_fusion.1
  70.7 0.0 copy-start.4
  70.7 4.2 %multiply_reduce_fusion = (f32[128]{0:T(128)S(1)}, f32[128,2048]{1,0:T(8,128)S(1)}) fusion(bf16[1024,2048]{1,0:T(8,128)(2,1)} %param.23, bf16[1024,1024]{1,0:T(8,128)(2,1)} %param.22, bf16[128,512]{1,0:T(8,128)(2,1)S(1)} %get-tuple-element.16, bf16[128,512]{1,0:T(8,128)(2,1)S(1)} %get-tuple-element.15, bf16[128,2048]{1,0:T(8,128)(2,1)} %param.24), kind=kOutput, calls=%fused_computation.18 | convolution fusion | flops 808058752 | bytes 8126976 | tf_op jit(solution)/shard_map/dot_general | solution.py:267
  74.9 0.8 convolution_convert_fusion.1
  75.7 0.0 copy-start.6
  75.7 50.5 %all_to_all.10 = bf16[32,16,2048]{2,1,0:T(8,128)(2,1)S(1)} all-to-all(bf16[32,16,2048]{2,1,0:T(8,128)(2,1)S(1)} %bitcast.53), channel_id=1, replica_groups=mesh['sp'=16,'tp'=2] {'sp','tp'}, dimensions={0} | all-to-all | bytes 4194304 | tf_op jit(solution)/shard_map/all_to_all | solution.py:282
  126.3 1.3 copy-done.1
  127.6 2.2 %fusion.5 = f32[512,512]{1,0:T(8,128)} fusion(bf16[512,2048]{1,0:T(8,128)(2,1)S(1)} %bitcast.55, bf16[1,2048,512]{2,1,0:T(8,128)(2,1)S(1)} %copy-done.6), kind=kOutput, calls=%fused_computation.9 | convolution fusion | flops 1073741824 | bytes 5242880 | tf_op jit(solution)/shard_map/dot_general | solution.py:237
  129.8 6.3 %convolution_convert_fusion = bf16[512,2048]{1,0:T(8,128)(2,1)} fusion(bf16[1,512,2048]{2,1,0:T(8,128)(2,1)S(1)} %copy-done, bf16[512,2048]{1,0:T(8,128)(2,1)} %bitcast.56, bf16[1,2048,512]{2,1,0:T(8,128)(2,1)} %param.29, f32[512,512]{1,0:T(8,128)} %fusion.5), kind=kOutput, calls=%fused_computation | convolution fusion | flops 2150105088 | bytes 9437184 | tf_op jit(solution)/shard_map/dot_general | solution.py:240
  136.1 3.7 %all-to-all-start.1 = ((bf16[32,16,2048]{2,1,0:T(8,128)(2,1)}), bf16[32,16,2048]{2,1,0:T(8,128)(2,1)}, u32[]{:S(2)}, u32[]{:S(2)}) async-start(bf16[32,16,2048]{2,1,0:T(8,128)(2,1)} %bitcast.54), calls=%async_computation.1 | async-start | bytes 4194304 | tf_op jit(solution)/shard_map/all_to_all | solution.py:286
  139.8 0.0 copy-done.5
  139.8 0.1 select_reduce_fusion
  140.0 48.6 %all-to-all-done.1 = bf16[32,16,2048]{2,1,0:T(8,128)(2,1)} async-done(((bf16[32,16,2048]{2,1,0:T(8,128)(2,1)}), bf16[32,16,2048]{2,1,0:T(8,128)(2,1)}, u32[]{:S(2)}, u32[]{:S(2)}) %all-to-all-start.1) | async-done | bytes 2097184 | tf_op jit(solution)/shard_map/all_to_all | solution.py:286
  188.5 2.0 %fusion.34 = f32[128,2048]{1,0:T(8,128)S(1)} fusion(bf16[512,2048]{1,0:T(8,128)(2,1)} %bitcast.12, f32[128,512]{1,0:T(8,128)S(1)} %select_reduce_fusion), kind=kOutput, calls=%fused_computation.42 | convolution fusion | flops 268500992 | bytes 3407872 | tf_op jit(solution)/shard_map/dot_general | solution.py:291
  190.6 2.9 %fusion.1 = bf16[128,2048]{1,0:T(8,128)(2,1)} fusion(f32[128,2048]{1,0:T(8,128)S(1)} %get-tuple-element.22, f32[128,2048]{1,0:T(8,128)S(1)} %fusion.34, bf16[512,2048]{1,0:T(8,128)(2,1)} %bitcast.12, f32[128,512]{1,0:T(8,128)S(1)} %select_reduce_fusion), kind=kOutput, calls=%fused_computation.5 | convolution fusion | flops 269484032 | bytes 4980736 | tf_op jit(solution)/shard_map/dot_general | solution.py:291
  (12 shorter events, 0.1 us)
Async XLA Ops:
  0.0 129.8 %copy-start = (bf16[1,512,2048]{2,1,0:T(8,128)(2,1)S(1)}, bf16[1,512,2048]{2,1,0:T(8,128)(2,1)}, u32[]{:S(2)}) copy-start(bf16[1,512,2048]{2,1,0:T(8,128)(2,1)} %param.30) | copy-start | bytes 6291460
  0.0 57.2 %copy-start.2 = (f32[32,128,16]{1,2,0:T(8,128)S(1)}, f32[32,128,16]{1,2,0:T(8,128)}, u32[]{:S(2)}) copy-start(f32[32,128,16]{1,2,0:T(8,128)} %param.20) | copy-start | bytes 786436
  59.2 9.2 %copy-start.3 = (s32[128,2]{0,1:T(2,128)S(1)}, s32[128,2]{0,1:T(2,128)}, u32[]{:S(2)}) copy-start(s32[128,2]{0,1:T(2,128)} %param.26) | copy-start | bytes 3076
  68.3 1.4 collective-permute-start
  70.7 4.2 %copy-start.4 = (f32[2048]{0:T(1024)S(1)}, f32[2048]{0:T(1024)}, u32[]{:S(2)}) copy-start(f32[2048]{0:T(1024)} %param.25) | copy-start | bytes 24580
  75.7 51.9 %copy-start.6 = (bf16[1,2048,512]{2,1,0:T(8,128)(2,1)S(1)}, bf16[1,2048,512]{2,1,0:T(8,128)(2,1)}, u32[]{:S(2)}) copy-start(bf16[1,2048,512]{2,1,0:T(8,128)(2,1)} %param.28) | copy-start | bytes 6291460
  126.3 1.3 copy-start.1
  136.1 3.7 %copy-start.5 = (f32[128,2]{0,1:T(2,128)S(1)}, f32[128,2]{0,1:T(2,128)}, u32[]{:S(2)}) copy-start(f32[128,2]{0,1:T(2,128)} %param.27) | copy-start | bytes 3076
  136.1 52.4 %all-to-all-start.1 = ((bf16[32,16,2048]{2,1,0:T(8,128)(2,1)}), bf16[32,16,2048]{2,1,0:T(8,128)(2,1)}, u32[]{:S(2)}, u32[]{:S(2)}) async-start(bf16[32,16,2048]{2,1,0:T(8,128)(2,1)} %bitcast.54), calls=%async_computation.1 | async-start | bytes 4194304 | tf_op jit(solution)/shard_map/all_to_all | solution.py:286

commit v2 on v1

v2 whole, which is shorter than its diff:
```python
import functools

import jax
import jax.numpy as jnp
from jax import lax
from jax.experimental import pallas as pl
from jax.experimental.pallas import tpu as pltpu
from jax.sharding import PartitionSpec as P

GROUPS = 4
EPSILON = 1e-06
LANES = 128
SEGMENTS = 8


def discretize(lam_real, lam_imag, state_in):
    magnitude = jnp.exp(lam_real)
    decay_re = magnitude * jnp.cos(lam_imag)
    decay_im = magnitude * jnp.sin(lam_imag)
    numer_re = decay_re - 1.0
    denom = lam_real * lam_real + lam_imag * lam_imag
    hold_re = ((numer_re * lam_real + decay_im * lam_imag) / denom)[:, None, :]
    hold_im = ((decay_im * lam_real - numer_re * lam_imag) / denom)[:, None, :]
    drive_re = hold_re * state_in[0] - hold_im * state_in[1]
    drive_im = hold_re * state_in[1] + hold_im * state_in[0]
    return drive_re.astype(jnp.bfloat16), drive_im.astype(jnp.bfloat16)


def powers(lam_real, lam_imag, exponent):
    magnitude = jnp.exp(exponent[:, None, None] * lam_real[None])
    angle = exponent[:, None, None] * lam_imag[None]
    return (magnitude * jnp.cos(angle), magnitude * jnp.sin(angle))


def iota(shape, dim):
    return lax.broadcasted_iota(jnp.int32, shape, dim)


def times(a_re, a_im, b_re, b_im):
    return a_re * b_re - a_im * b_im, a_re * b_im + a_im * b_re


def segment_order(rows, back=False):
    length = rows // SEGMENTS
    ordered, token = iota((rows, rows), 1 if back else 0), iota((rows, rows), 0 if back else 1)
    same = (ordered % SEGMENTS) * length + ordered // SEGMENTS == token
    return same.astype(jnp.float32).astype(jnp.bfloat16)


def spread(block, copies, row_group, column_group):
    rows, width = block.shape
    wide = width * copies
    pick = iota((width, wide), 0) == iota((width, wide), 1) % width
    tiled = jnp.dot(
        block, pick.astype(jnp.float32).astype(jnp.bfloat16), preferred_element_type=jnp.float32
    )
    keep = (iota((rows, wide), 0) // row_group) == (iota((rows, wide), 1) // column_group)
    return jnp.where(keep, tiled, 0.0).astype(jnp.bfloat16)


def ssm_ordered(x_ref):
    rows = x_ref.shape[0]
    return jnp.dot(
        segment_order(rows), x_ref[...], preferred_element_type=jnp.float32
    )


def fill_push(x_tile, drive_re_ref, drive_im_ref, tile, channels, push):
    states = drive_re_ref.shape[1]
    copies = LANES // channels
    width = copies * states
    rows = pl.ds(tile * LANES, LANES)
    for part, ref in enumerate((drive_re_ref, drive_im_ref)):
        block = spread(ref[rows, :], copies, channels, states)
        push[:, part * width : (part + 1) * width] = jnp.dot(
            x_tile, block, preferred_element_type=jnp.float32
        )


def run_scan(push, width, decay_re, decay_im, start_re, start_im, keep):
    shape = (SEGMENTS, width)
    decay_re = jnp.broadcast_to(decay_re, shape)
    decay_im = jnp.broadcast_to(decay_im, shape)

    def step(j, carry):
        rows = pl.ds(pl.multiple_of(j * SEGMENTS, SEGMENTS), SEGMENTS)
        next_re, next_im = times(decay_re, decay_im, *carry)
        next_re = next_re + push[rows, :width]
        next_im = next_im + push[rows, width:]
        if keep:
            push[rows, :width] = next_re
            push[rows, width:] = next_im
        return next_re, next_im

    return lax.fori_loop(0, push.shape[0] // SEGMENTS, step, (start_re, start_im), unroll=4)


MESH = pl.DeviceIdType.MESH


def mixer_kernel(channels, sp_count, x_ref, drive_re_ref, drive_im_ref, pow_re_ref, pow_im_ref,
                 read_ref, skip_ref, out_ref, push, start, pre, ends_re, ends_im, final, finals,
                 halves, taken, send_sem, recv_sem, swap_sem):
    mine, core = lax.axis_index("sp"), lax.axis_index("tp")

    def peer(step):
        return (lax.rem(mine + step, sp_count), core)

    barrier = pltpu.get_barrier_semaphore()

    @pl.loop(1, sp_count)
    def _(step):
        pl.semaphore_signal(barrier, inc=1, device_id=peer(step), device_id_type=MESH)

    pl.semaphore_signal(barrier, inc=1, device_id=(mine, 1 - core), device_id_type=MESH)

    wide = ssm_ordered(x_ref)
    ordered = wide.astype(jnp.bfloat16)
    rows = x_ref.shape[0]
    width = push.shape[2] // 2
    total = pow_re_ref.shape[1]
    states = drive_re_ref.shape[1]
    copies = LANES // channels
    for tile in range(total // width):
        lanes = slice(tile * width, (tile + 1) * width)
        fill_push(
            ordered[:, tile * LANES : (tile + 1) * LANES], drive_re_ref, drive_im_ref, tile,
            channels, push.at[tile],
        )
        zero = jnp.zeros((SEGMENTS, width), jnp.float32)
        end_re, end_im = run_scan(
            push.at[tile], width, pow_re_ref[0:1, lanes], pow_im_ref[0:1, lanes], zero, zero,
            False,
        )
        ends_re[:, lanes] = end_re
        ends_im[:, lanes] = end_im
        seg_re, seg_im = pow_re_ref[1:2, lanes], pow_im_ref[1:2, lanes]
        sum_re, sum_im = end_re[0:1], end_im[0:1]
        for s in range(1, SEGMENTS):
            sum_re, sum_im = times(seg_re, seg_im, sum_re, sum_im)
            sum_re, sum_im = sum_re + end_re[s : s + 1], sum_im + end_im[s : s + 1]
        final[0:1, lanes] = sum_re
        final[1:2, lanes] = sum_im

    pl.semaphore_wait(barrier, sp_count)

    def give(step):
        return pltpu.make_async_remote_copy(
            src_ref=final, dst_ref=finals.at[mine], send_sem=send_sem.at[step],
            recv_sem=recv_sem.at[step], device_id=peer(step), device_id_type=MESH,
        )

    @pl.loop(1, sp_count)
    def _(step):
        give(step).start()

    @pl.loop(1, sp_count)
    def _(step):
        give(step).wait()

    for tile in range(total // width):
        lanes = slice(tile * width, (tile + 1) * width)
        span_re, span_im = pow_re_ref[2:3, lanes], pow_im_ref[2:3, lanes]
        zero = jnp.zeros((1, width), jnp.float32)

        def hop(position, so_far):
            new_re, new_im = times(span_re, span_im, *so_far)
            return (new_re + finals[position, 0:1, lanes], new_im + finals[position, 1:2, lanes])

        in_re, in_im = lax.fori_loop(0, mine, hop, (zero, zero))
        seg_re, seg_im = pow_re_ref[1:2, lanes], pow_im_ref[1:2, lanes]
        for s in range(SEGMENTS):
            start[s : s + 1, :width] = in_re
            start[s : s + 1, width:] = in_im
            in_re, in_im = times(seg_re, seg_im, in_re, in_im)
            in_re = in_re + ends_re[s : s + 1, lanes]
            in_im = in_im + ends_im[s : s + 1, lanes]
        own = slice(tile * LANES, (tile + 1) * LANES)
        run_scan(
            push.at[tile], width, pow_re_ref[0:1, lanes], pow_im_ref[0:1, lanes],
            start[:, :width], start[:, width:], True,
        )
        read = jnp.zeros((rows, LANES), jnp.float32)
        for part in range(2):
            block = read_ref[tile * copies : (tile + 1) * copies,
                             part * states : (part + 1) * states, :]
            block = block.reshape(width, channels).astype(jnp.bfloat16)
            block = spread(block, copies, states, channels)
            read = read + jnp.dot(
                push[tile, :, part * width : (part + 1) * width].astype(jnp.bfloat16), block,
                preferred_element_type=jnp.float32,
            )
        value = jax.nn.gelu(read + skip_ref[0:1, own] * wide[:, own])
        pre[:, own] = value.astype(jnp.bfloat16)
    half = rows // 2
    back = jnp.dot(
        segment_order(rows, back=True), pre[...], preferred_element_type=jnp.float32
    ).astype(jnp.bfloat16)
    halves[0] = back[:half]
    halves[1] = back[half:]
    swap = pltpu.make_async_remote_copy(
        src_ref=halves.at[1 - core], dst_ref=taken, send_sem=swap_sem.at[0],
        recv_sem=swap_sem.at[1], device_id=(mine, 1 - core), device_id_type=MESH,
    )
    swap.start()
    wide_in = x_ref.shape[1]
    out_ref[:, pl.ds(pl.multiple_of(core * wide_in, LANES), wide_in)] = halves[core]
    swap.wait()
    out_ref[:, pl.ds(pl.multiple_of((1 - core) * wide_in, LANES), wide_in)] = taken[...]


def mixer(ssm_input, lam_real, lam_imag, state_in, read_out, channel_skip):
    rows, width_in = ssm_input.shape
    groups, states = lam_real.shape
    channels = state_in.shape[2]
    sp_count = lax.axis_size("sp")
    total = groups * states
    width = (LANES // channels) * states
    drive_re, drive_im = discretize(lam_real, lam_imag, state_in)
    drive_re = drive_re.reshape(width_in, states)
    drive_im = drive_im.reshape(width_in, states)
    steps = jnp.asarray([1.0, rows // SEGMENTS, rows], jnp.float32)
    pow_re, pow_im = powers(lam_real, lam_imag, steps)
    pow_re, pow_im = pow_re.reshape(3, total), pow_im.reshape(3, total)
    f32, bf16 = jnp.float32, jnp.bfloat16
    return pl.pallas_call(
        functools.partial(mixer_kernel, channels, sp_count),
        out_shape=jax.ShapeDtypeStruct((rows // 2, width_in * 2), bf16),
        scratch_shapes=[
            pltpu.VMEM((total // width, rows, 2 * width), f32),
            pltpu.VMEM((SEGMENTS, 2 * width), f32),
            pltpu.VMEM((rows, width_in), bf16),
            pltpu.VMEM((SEGMENTS, total), f32),
            pltpu.VMEM((SEGMENTS, total), f32),
            pltpu.VMEM((2, total), f32),
            pltpu.VMEM((sp_count, 2, total), f32),
            pltpu.VMEM((2, rows // 2, width_in), bf16),
            pltpu.VMEM((rows // 2, width_in), bf16),
            pltpu.SemaphoreType.DMA((sp_count,)),
            pltpu.SemaphoreType.DMA((sp_count,)),
            pltpu.SemaphoreType.DMA((2,)),
        ],
        compiler_params=pltpu.CompilerParams(collective_id=0, has_side_effects=True),
        name="mixer",
    )(ssm_input, drive_re, drive_im, pow_re, pow_im, read_out, channel_skip.reshape(1, width_in))


def place(meta, slots, weigh):
    tokens = meta.shape[1]
    slot = iota((slots, tokens), 0).astype(jnp.float32)
    total = jnp.zeros((slots, tokens), jnp.float32)
    for k in range(2):
        value = meta[2 + k : 3 + k] if weigh else 1.0
        total = total + jnp.where(slot == meta[k : k + 1], value, 0.0)
    return total


def experts_kernel(planes, members, cores, rows_ref, meta_ref, mixed_ref, gather_ref,
                   gate_hbm, up_hbm, down_hbm, out_ref, gate, up, down, got, got_meta, sent,
                   arrived, answer, back, joined, home, load_sem, z_send, z_recv, m_send, m_recv,
                   out_send, out_recv, ret_send, ret_recv, home_send, home_recv):
    f32, bf16 = jnp.float32, jnp.bfloat16
    loads = [
        pltpu.make_async_copy(hbm.at[0], vmem, load_sem.at[i])
        for i, (hbm, vmem) in enumerate(((gate_hbm, gate), (up_hbm, up), (down_hbm, down)))
    ]
    for load in loads:
        load.start()
    sp, core = lax.axis_index("sp"), lax.axis_index("tp")
    per_plane = members // cores
    plane = sp // per_plane
    column = sp - plane * per_plane
    member = column * cores + core

    def plane_at(step):
        return lax.rem(plane + step, planes)

    def above(step):
        return (plane_at(step) * per_plane + column, core)

    def member_at(step):
        return lax.rem(member + step, members)

    def beside(step):
        other = member_at(step)
        return (plane * per_plane + other // cores, lax.rem(other, cores))

    barrier = pltpu.get_barrier_semaphore()

    @pl.loop(1, planes)
    def _(step):
        pl.semaphore_signal(barrier, inc=1, device_id=above(step), device_id_type=MESH)

    @pl.loop(1, members)
    def _(step):
        pl.semaphore_signal(barrier, inc=1, device_id=beside(step), device_id_type=MESH)

    pl.semaphore_wait(barrier, planes + members - 2)

    def remote(src, dst, send, recv, where):
        return pltpu.make_async_remote_copy(
            src_ref=src, dst_ref=dst, send_sem=send, recv_sem=recv, device_id=where,
            device_id_type=MESH,
        )

    def meta_copy(d):
        return remote(meta_ref.at[plane_at(d)], got_meta.at[d], m_send.at[d], m_recv.at[d],
                      above(d))

    def rows_copy(d):
        return remote(rows_ref.at[plane_at(d)], got.at[d], z_send.at[d], z_recv.at[d], above(d))

    def out_copy(d, step):
        return remote(sent.at[d, member_at(step)], arrived.at[d, member], out_send.at[d, step],
                      out_recv.at[d, step], beside(step))

    def ret_copy(d, step):
        return remote(answer.at[d, member_at(step)], back.at[d, member], ret_send.at[d, step],
                      ret_recv.at[d, step], beside(step))

    def home_copy(d):
        return remote(joined.at[d], home.at[d], home_send.at[d], home_recv.at[d],
                      above(planes - d))

    for d in range(1, planes):
        meta_copy(d).start()
    for d in range(1, planes):
        rows_copy(d).start()

    capacity, model_width = sent.shape[2], sent.shape[3]
    slots = members * capacity
    tokens = rows_ref.shape[1]

    def dispatch(d):
        if d:
            meta_copy(d).wait_recv()
            rows_copy(d).wait_recv()
            block, meta = got[d], got_meta[d]
        else:
            block, meta = rows_ref[plane], meta_ref[plane]
        pick = place(meta[:, :tokens], slots, False).astype(bf16)
        spread_rows = jnp.dot(pick, block, preferred_element_type=f32).astype(bf16)
        sent[d] = spread_rows.reshape(members, capacity, model_width)

        @pl.loop(1, members)
        def _(step):
            out_copy(d, step).start()

        arrived[d, member] = sent[d, member]

    def expert(d):
        if d == 0:
            for load in loads:
                load.wait()

        @pl.loop(1, members)
        def _(step):
            out_copy(d, step).wait_recv()

        rows = arrived[d].reshape(slots, model_width)
        gate_part = jnp.dot(rows, gate[...], preferred_element_type=f32)
        up_part = jnp.dot(rows, up[...], preferred_element_type=f32)
        hidden = (jax.nn.silu(gate_part) * up_part).astype(bf16)
        result = jnp.dot(hidden, down[...], preferred_element_type=f32).astype(bf16)
        answer[d] = result.reshape(members, capacity, model_width)

        @pl.loop(1, members)
        def _(step):
            ret_copy(d, step).start()

        back[d, member] = answer[d, member]

    def join(d):
        @pl.loop(1, members)
        def _(step):
            ret_copy(d, step).wait_recv()

        meta = got_meta[d] if d else meta_ref[plane]
        weights = place(meta[:, :tokens], slots, True)
        coarse = weights.astype(bf16)
        fine = (weights - coarse.astype(f32)).astype(bf16)
        answers = back[d].reshape(slots, model_width)
        over_slots = (((0,), (0,)), ((), ()))
        total = lax.dot_general(coarse, answers, over_slots, preferred_element_type=f32)
        total = total + lax.dot_general(fine, answers, over_slots, preferred_element_type=f32)
        if d:
            joined[d] = total.astype(bf16)
            home_copy(d).start()
        else:
            home[0] = total.astype(bf16)

    dispatch(0)
    expert(0)
    for d in range(1, planes):
        dispatch(d)
        expert(d)
        join(d - 1)
    join(planes - 1)

    total = mixed_ref[...]
    for d in range(planes):
        if d:
            home_copy(d).wait_recv()
        total = total + jnp.dot(
            gather_ref[plane_at(d)], home[d], preferred_element_type=f32
        )
    out_ref[...] = total.astype(bf16)

    for d in range(1, planes):
        meta_copy(d).wait_send()
        rows_copy(d).wait_send()
        home_copy(d).wait_send()

    for d in range(planes):
        @pl.loop(1, members)
        def _(step):
            out_copy(d, step).wait_send()
            ret_copy(d, step).wait_send()


def earlier_count(onehot):
    tokens = onehot.shape[0]
    earlier = (jnp.arange(tokens)[:, None] > jnp.arange(tokens)[None, :]).astype(jnp.bfloat16)
    return jnp.dot(earlier, onehot.astype(jnp.bfloat16), preferred_element_type=jnp.float32)


def routes(expert_ids, route_weight, members, capacity, room, padded):
    tokens = expert_ids.shape[0]
    count = members * GROUPS
    f32 = jnp.float32
    onehot = (expert_ids[:, :, None] == jnp.arange(count, dtype=jnp.int32)).astype(f32)
    both = jnp.sum(onehot, axis=1)
    group = expert_ids[:, 0] // members
    in_group = (group[:, None] == jnp.arange(GROUPS, dtype=jnp.int32)).astype(f32)
    before = earlier_count(jnp.concatenate([both, in_group], axis=1))
    rank = jnp.sum(before[:, None, :count] * onehot, axis=-1)
    slot = (expert_ids - group[:, None] * members).astype(f32) * padded + rank
    row = group * room + jnp.sum(before[:, count:] * in_group, axis=1).astype(jnp.int32)
    mine = row[None, :] == jnp.arange(GROUPS * room, dtype=jnp.int32)[:, None]
    values = jnp.concatenate([slot + 1.0, route_weight], axis=1)
    meta = jnp.sum(jnp.where(mine[None], values.T[:, None, :], 0.0), axis=-1)
    meta = meta - jnp.asarray([1.0, 1.0, 0.0, 0.0], f32)[:, None]
    meta = meta.reshape(4, GROUPS, room).transpose(1, 0, 2)
    meta = jnp.pad(meta, ((0, 0), (0, 4), (0, -room % LANES)))
    return mine.astype(jnp.bfloat16), meta


def experts(normed, mixed, expert_ids, route_weight, expert_gate, expert_up, expert_down):
    f32, bf16 = jnp.float32, jnp.bfloat16
    tokens, model_width = normed.shape
    hidden = expert_gate.shape[2]
    cores = lax.axis_size("tp")
    members = lax.axis_size("sp") * cores // GROUPS
    capacity = tokens // members
    room = members * capacity // expert_ids.shape[1]
    padded = -(-capacity // 16) * 16
    mine, meta = routes(expert_ids, route_weight, members, capacity, room, padded)
    rows = jnp.dot(mine, normed, preferred_element_type=f32).astype(bf16)
    rows = rows.reshape(GROUPS, room, model_width)
    gather = mine.reshape(GROUPS, room, tokens).transpose(0, 2, 1)
    vmem = pl.BlockSpec(memory_space=pltpu.VMEM)
    hbm = pl.BlockSpec(memory_space=pl.ANY)
    block = pltpu.VMEM((GROUPS, members, padded, model_width), bf16)
    group_rows = pltpu.VMEM((GROUPS, room, model_width), bf16)
    dma = pltpu.SemaphoreType.DMA
    return pl.pallas_call(
        functools.partial(experts_kernel, GROUPS, members, cores),
        out_shape=jax.ShapeDtypeStruct((tokens, model_width), bf16),
        in_specs=[vmem] * 4 + [hbm] * 3,
        out_specs=vmem,
        scratch_shapes=[
            pltpu.VMEM((model_width, hidden), bf16),
            pltpu.VMEM((model_width, hidden), bf16),
            pltpu.VMEM((hidden, model_width), bf16),
            group_rows,
            pltpu.VMEM(meta.shape, f32),
            block, block, block, block,
            group_rows, group_rows,
            dma((3,)),
            dma((GROUPS,)), dma((GROUPS,)), dma((GROUPS,)), dma((GROUPS,)),
            dma((GROUPS, members)), dma((GROUPS, members)),
            dma((GROUPS, members)), dma((GROUPS, members)),
            dma((GROUPS,)), dma((GROUPS,)),
        ],
        compiler_params=pltpu.CompilerParams(collective_id=1, has_side_effects=True),
        name="experts",
    )(rows, meta, mixed, gather, expert_gate, expert_up, expert_down)


def on_device(
    ssm_input,
    lam_real,
    lam_imag,
    state_in,
    read_out,
    channel_skip,
    glu_weight,
    out_weight,
    residual,
    norm_gain,
    expert_ids,
    route_weight,
    expert_gate,
    expert_up,
    expert_down,
):
    f32, bf16 = jnp.float32, jnp.bfloat16
    own_tokens = mixer(ssm_input, lam_real, lam_imag, state_in, read_out, channel_skip)
    gate_lin = jnp.dot(own_tokens, glu_weight, preferred_element_type=f32)
    gated = (own_tokens.astype(f32) * jax.nn.sigmoid(gate_lin)).astype(bf16)
    mixed = residual.astype(f32) + jnp.dot(gated, out_weight, preferred_element_type=f32)
    normed = (
        mixed * lax.rsqrt(jnp.mean(mixed * mixed, axis=-1, keepdims=True) + EPSILON) * norm_gain
    ).astype(bf16)
    return experts(
        normed, mixed, expert_ids, route_weight, expert_gate, expert_up, expert_down
    )


def solution(mesh):
    placed = (
        P("sp", "tp"),
        P("tp", None),
        P("tp", None),
        P(None, "tp", None, None),
        P("tp", None, None),
        P("tp"),
        P(),
        P(),
        P(("sp", "tp"), None),
        P(),
        P(("sp", "tp"), None),
        P(("sp", "tp"), None),
        P(("sp", "tp"), None, None),
        P(("sp", "tp"), None, None),
        P(("sp", "tp"), None, None),
    )
    return jax.shard_map(
        on_device, mesh=mesh, in_specs=placed, out_specs=P(("sp", "tp"), None), check_vma=False
    )
```

time: 194 us -> 115 us (0.59)
  blocking collectives: 96.9 us -> 0 us
  Pallas kernels: 13.1 us -> 97.3 us
  waiting for transfers between devices: 49.5 us -> 0 us
  matrix products: 18.5 us -> 5.35 us
  starting transfers between devices: 3.79 us -> 0 us
    pallas_call x2, Pallas kernels: 13.1 us -> 97.3 us  [the longest x1 77.1 us: experts(): pl.pallas_call(functools.partial(experts_kernel, GROUPS, members, cores),...]
    all_to_all x1 -> x0, blocking collectives: 50.5 us -> none  [on_device(): lax.all_to_all(outgoing, ('sp', 'tp'), split_axis=0, concat_axis=0, tiled...]
    all_to_all x1 -> x0, waiting for transfers between devices: 48.6 us -> none  [on_device(): lax.all_to_all(answered, ('sp', 'tp'), split_axis=0, concat_axis=0, tiled...]
    all_gather x1 -> x0, blocking collectives: 46.3 us -> none  [mixer(): finals = lax.all_gather(final, 'sp')]
    dot_general x6 -> x2, matrix products: 14.4 us -> 1.64 us  [the longest x1 1.51 us: experts(): rows = jnp.dot(mine, normed, preferred_element_type=f32).astype(bf16)]
    all_to_all x1 -> x0, starting transfers between devices: 3.72 us -> none  [on_device(): lax.all_to_all(answered, ('sp', 'tp'), split_axis=0, concat_axis=0, tiled...]
    unnamed x15 -> x16, local copies, waits for them, and re-layouts: 3.28 us -> 3.88 us
  transfers between devices with their start and end apart: 2 -> 0, of which waited for: 2 -> 0; matrix products, arithmetic and copies ran while one was open for 0% -> 0% of each run, Pallas kernels for 0% -> 0%
where the time goes in v2:
time: 115 us
  Pallas kernels  97.3 us (85%)
  local copies, waits for them, and re-layouts  7.37 us (6%)
  matrix products  5.35 us (5%)
  other arithmetic  4.37 us (4%)
    pallas_call x1, Pallas kernels, experts(): pl.pallas_call(functools.partial(experts_kernel, GROUPS, members, cores),...  77.1 us
    pallas_call x1, Pallas kernels, mixer(): pl.pallas_call(functools.partial(mixer_kernel, channels, sp_count), out_s...  20.2 us
    unnamed x16, local copies, waits for them, and re-layouts  3.88 us
    dot_general x1, matrix products, on_device(): jnp.dot(gated, out_weight, preferred_element_type=f32)  3.7 us

profile of v2, /device:TPU:0, one launch (start us, length us, event | category | flops | bytes accessed | tf_op | source)
XLA Modules:
  0.0 114.6 jit_solution(8684474775008110622)
XLA Ops:
  0.0 0.0 copy-start
  0.0 0.0 copy-start.2
  0.0 1.2 %fusion.26 = (f32[1,32,16,64]{3,2,1,0:T(8,128)S(1)}, f32[1,32,16,64]{3,2,1,0:T(8,128)S(1)}) fusion(f32[2,32,16,64]{3,2,1,0:T(8,128)} %param.20), kind=kLoop, calls=%fused_computation.68 | loop fusion | bytes 524288 | tf_op jit(solution)/shard_map/slice | solution.py:24
  1.2 0.8 fusion.16
  2.1 0.8 fusion.11
  2.8 0.8 mul.177
  3.6 0.8 mul.180
  4.4 1.6 %fusion.15 = (f32[3,2048]{1,0:T(4,128)}, f32[3,2048]{1,0:T(4,128)}) fusion(f32[2048]{0:T(1024)S(1)} %mul.180, f32[2048]{0:T(1024)S(1)} %mul.177, f32[3]{0:T(128)} %constant.44.clone), kind=kLoop, calls=%fused_computation.30 | loop fusion | flops 24576 | bytes 65548 | tf_op jit(solution)/shard_map/mul | solution.py:32
  6.0 0.0 copy-done.2
  6.0 2.0 %copy.31.read_ref = f32[32,128,16]{2,1,0:T(8,128)} copy(f32[32,128,16]{1,2,0:T(8,128)S(1)} %copy-done.2) | data formatting | bytes 524288 | tf_op args[4]
  7.9 20.2 %mixer.1 = bf16[128,1024]{1,0:T(8,128)(2,1)} custom-call(bf16[256,512]{1,0:T(8,128)(2,1)} %x_ref.1, bf16[512,64]{1,0:T(8,128)(2,1)} %get-tuple-element.8.drive_re_ref, bf16[512,64]{1,0:T(8,128)(2,1)} %get-tuple-element.7.drive_im_ref, f32[3,2048]{1,0:T(4,128)} %get-tuple-element.14.pow_re_ref, f32[3,2048]{1,0:T(4,128)} %get-tuple-element.13.pow_im_ref, ...), custom_call_target="tpu_custom_call" | custom-call | tf_op jit(solution)/shard_map/mixer/pallas_call | solution.py:226
  28.2 0.0 copy-done
  28.2 0.0 copy-start.3
  28.2 0.0 copy-start.4
  28.2 3.7 %multiply_reduce_fusion = (f32[128]{0:T(128)S(1)}, f32[128,2048]{1,0:T(8,128)S(1)}) fusion(bf16[1024,2048]{1,0:T(8,128)(2,1)} %param.24, bf16[128,1024]{1,0:T(8,128)(2,1)} %mixer.1, bf16[1024,1024]{1,0:T(8,128)(2,1)S(1)} %copy-done, bf16[128,2048]{1,0:T(8,128)(2,1)} %param.25), kind=kOutput, calls=%fused_computation.9 | convolution fusion | flops 807141248 | bytes 8126976 | tf_op jit(solution)/shard_map/dot_general | solution.py:511
  31.9 0.0 copy-start.1
  31.9 0.0 copy-start.5
  31.9 0.0 copy-start.6
  32.0 0.0 copy-done.3
  32.0 0.1 fusion.13
  32.2 0.0 copy-done.4
  32.2 1.5 %convolution_convert_fusion = bf16[256,2048]{1,0:T(8,128)(2,1)} fusion(f32[128,2048]{1,0:T(8,128)S(1)} %get-tuple-element.16.mixed_ref, f32[2048]{0:T(1024)S(1)} %copy-done.4, f32[128]{0:T(128)S(1)} %add_rsqrt_fusion, s32[128]{0:T(128)S(1)} %convert_add_fusion), kind=kOutput, calls=%fused_computation | convolution fusion | flops 135561216 | bytes 2106368 | tf_op jit(solution)/shard_map/dot_general | solution.py:458
  33.8 0.0 copy-done.5
  33.8 0.2 select_reduce_fusion
  34.0 0.1 reduce_sum.52
  34.1 0.0 copy-done.6
  34.1 0.1 fusion.22
  34.2 0.6 pad.4.meta_ref
  34.8 0.8 compare_convert_fusion.gather_ref
  35.6 0.0 copy-done.1
  35.6 77.1 %experts.1 = bf16[128,2048]{1,0:T(8,128)(2,1)} custom-call(bf16[4,64,2048]{2,1,0:T(8,128)(2,1)} %bitcast.46, f32[4,8,128]{2,1,0:T(8,128)} %pad.4.meta_ref, f32[128,2048]{1,0:T(8,128)} %copy-done.1, bf16[4,128,64]{2,1,0:T(8,128)(2,1)} %compare_convert_fusion.gather_ref, bf16[1,2048,512]{2,1,0:T(8,128)(2,1)} %gate_hbm.1, bf16[1,2048,512]{2,1,0:T(8,128)(2,1)} %up_hbm.1, ...), custom_call_target="tpu_custom_call" | custom-call | tf_op jit(solution)/shard_map/experts/pallas_call | solution.py:466
  112.7 1.9 %copy.37 = bf16[128,2048]{1,0:T(8,128)(2,1)} copy(bf16[128,2048]{1,0:T(8,128)(2,1)} %experts.1) | data formatting | bytes 1048576
  (12 shorter events, 0.2 us)
Async XLA Ops:
  0.0 28.2 %copy-start = (bf16[1024,1024]{1,0:T(8,128)(2,1)S(1)}, bf16[1024,1024]{1,0:T(8,128)(2,1)}, u32[]{:S(2)}) copy-start(bf16[1024,1024]{1,0:T(8,128)(2,1)} %param.23) | copy-start | bytes 6291460
  0.0 6.0 %copy-start.2 = (f32[32,128,16]{1,2,0:T(8,128)S(1)}, f32[32,128,16]{1,2,0:T(8,128)}, u32[]{:S(2)}) copy-start(f32[32,128,16]{1,2,0:T(8,128)} %param.21) | copy-start | bytes 786436
  28.2 3.8 %copy-start.3 = (s32[128,2]{0,1:T(2,128)S(1)}, s32[128,2]{0,1:T(2,128)}, u32[]{:S(2)}) copy-start(s32[128,2]{0,1:T(2,128)} %param.27) | copy-start | bytes 3076
  28.2 4.0 %copy-start.4 = (f32[2048]{0:T(1024)S(1)}, f32[2048]{0:T(1024)}, u32[]{:S(2)}) copy-start(f32[2048]{0:T(1024)} %param.26) | copy-start | bytes 24580
  31.9 3.7 %copy-start.1 = (f32[128,2048]{1,0:T(8,128)}, f32[128,2048]{1,0:T(8,128)S(1)}, u32[]{:S(2)}) copy-start(f32[128,2048]{1,0:T(8,128)S(1)} %get-tuple-element.16.mixed_ref) | copy-start | bytes 3145732
  31.9 1.9 %copy-start.5 = (f32[128,2]{0,1:T(2,128)S(1)}, f32[128,2]{0,1:T(2,128)}, u32[]{:S(2)}) copy-start(f32[128,2]{0,1:T(2,128)} %param.28) | copy-start | bytes 3076
  31.9 2.2 %copy-start.6 = (f32[4]{0:T(128)S(1)}, f32[4]{0:T(128)}, u32[]{:S(2)}) copy-start(f32[4]{0:T(128)} %constant.51) | copy-start | bytes 52

commit v3 on v2

--- a/solution.py
+++ b/solution.py
@@ -389,13 +389,13 @@
         else:
             home[0] = total.astype(bf16)
 
-    dispatch(0)
-    expert(0)
-    for d in range(1, planes):
-        dispatch(d)
-        expert(d)
-        join(d - 1)
-    join(planes - 1)
+    for d in range(planes + 2):
+        if d < planes:
+            dispatch(d)
+        if 1 <= d <= planes:
+            expert(d - 1)
+        if d >= 2:
+            join(d - 2)
 
     total = mixed_ref[...]
     for d in range(planes):

time: 115 us -> 109 us (0.948)
  Pallas kernels: 97.3 us -> 91.1 us
    pallas_call x1, Pallas kernels: 77.1 us -> 70.9 us  [experts(): pl.pallas_call(functools.partial(experts_kernel, GROUPS, members, cores),...]
where the time goes in v3:
time: 109 us; the launch traced here: 108 us
  Pallas kernels  91.1 us (84%)
  local copies, waits for them, and re-layouts  7.37 us (7%)
  matrix products  5.35 us (5%)
  other arithmetic  4.37 us (4%)
    pallas_call x1, Pallas kernels, experts(): pl.pallas_call(functools.partial(experts_kernel, GROUPS, members, cores),...  70.9 us
    pallas_call x1, Pallas kernels, mixer(): pl.pallas_call(functools.partial(mixer_kernel, channels, sp_count), out_s...  20.2 us
    unnamed x16, local copies, waits for them, and re-layouts  3.88 us
    dot_general x1, matrix products, on_device(): jnp.dot(gated, out_weight, preferred_element_type=f32)  3.7 us

profile of v3, /device:TPU:0, one launch (start us, length us, event | category | flops | bytes accessed | tf_op | source)
XLA Modules:
  0.0 108.4 jit_solution(16428736513810502272)
XLA Ops:
  0.0 0.0 copy-start
  0.0 0.0 copy-start.2
  0.0 1.2 %fusion.26 = (f32[1,32,16,64]{3,2,1,0:T(8,128)S(1)}, f32[1,32,16,64]{3,2,1,0:T(8,128)S(1)}) fusion(f32[2,32,16,64]{3,2,1,0:T(8,128)} %param.20), kind=kLoop, calls=%fused_computation.68 | loop fusion | bytes 524288 | tf_op jit(solution)/shard_map/slice | solution.py:24
  1.2 0.8 fusion.16
  2.1 0.8 fusion.11
  2.8 0.8 mul.177
  3.6 0.8 mul.180
  4.4 1.6 %fusion.15 = (f32[3,2048]{1,0:T(4,128)}, f32[3,2048]{1,0:T(4,128)}) fusion(f32[2048]{0:T(1024)S(1)} %mul.180, f32[2048]{0:T(1024)S(1)} %mul.177, f32[3]{0:T(128)} %constant.44.clone), kind=kLoop, calls=%fused_computation.30 | loop fusion | flops 24576 | bytes 65548 | tf_op jit(solution)/shard_map/mul | solution.py:32
  6.0 0.0 copy-done.2
  6.0 2.0 %copy.31.read_ref = f32[32,128,16]{2,1,0:T(8,128)} copy(f32[32,128,16]{1,2,0:T(8,128)S(1)} %copy-done.2) | data formatting | bytes 524288 | tf_op args[4]
  7.9 20.2 %mixer.1 = bf16[128,1024]{1,0:T(8,128)(2,1)} custom-call(bf16[256,512]{1,0:T(8,128)(2,1)} %x_ref.1, bf16[512,64]{1,0:T(8,128)(2,1)} %get-tuple-element.8.drive_re_ref, bf16[512,64]{1,0:T(8,128)(2,1)} %get-tuple-element.7.drive_im_ref, f32[3,2048]{1,0:T(4,128)} %get-tuple-element.14.pow_re_ref, f32[3,2048]{1,0:T(4,128)} %get-tuple-element.13.pow_im_ref, ...), custom_call_target="tpu_custom_call" | custom-call | tf_op jit(solution)/shard_map/mixer/pallas_call | solution.py:226
  28.2 0.0 copy-done
  28.2 0.0 copy-start.3
  28.2 0.0 copy-start.4
  28.2 3.7 %multiply_reduce_fusion = (f32[128]{0:T(128)S(1)}, f32[128,2048]{1,0:T(8,128)S(1)}) fusion(bf16[1024,2048]{1,0:T(8,128)(2,1)} %param.24, bf16[128,1024]{1,0:T(8,128)(2,1)} %mixer.1, bf16[1024,1024]{1,0:T(8,128)(2,1)S(1)} %copy-done, bf16[128,2048]{1,0:T(8,128)(2,1)} %param.25), kind=kOutput, calls=%fused_computation.9 | convolution fusion | flops 807141248 | bytes 8126976 | tf_op jit(solution)/shard_map/dot_general | solution.py:511
  31.9 0.0 copy-start.1
  31.9 0.0 copy-start.5
  31.9 0.0 copy-start.6
  32.0 0.0 copy-done.3
  32.0 0.1 fusion.13
  32.2 0.0 copy-done.4
  32.2 1.5 %convolution_convert_fusion = bf16[256,2048]{1,0:T(8,128)(2,1)} fusion(f32[128,2048]{1,0:T(8,128)S(1)} %get-tuple-element.16.mixed_ref, f32[2048]{0:T(1024)S(1)} %copy-done.4, f32[128]{0:T(128)S(1)} %add_rsqrt_fusion, s32[128]{0:T(128)S(1)} %convert_add_fusion), kind=kOutput, calls=%fused_computation | convolution fusion | flops 135561216 | bytes 2106368 | tf_op jit(solution)/shard_map/dot_general | solution.py:458
  33.8 0.0 copy-done.5
  33.8 0.2 select_reduce_fusion
  34.0 0.1 reduce_sum.52
  34.1 0.0 copy-done.6
  34.1 0.1 fusion.22
  34.2 0.6 pad.4.meta_ref
  34.8 0.8 compare_convert_fusion.gather_ref
  35.6 0.0 copy-done.1
  35.6 70.9 %experts.1 = bf16[128,2048]{1,0:T(8,128)(2,1)} custom-call(bf16[4,64,2048]{2,1,0:T(8,128)(2,1)} %bitcast.46, f32[4,8,128]{2,1,0:T(8,128)} %pad.4.meta_ref, f32[128,2048]{1,0:T(8,128)} %copy-done.1, bf16[4,128,64]{2,1,0:T(8,128)(2,1)} %compare_convert_fusion.gather_ref, bf16[1,2048,512]{2,1,0:T(8,128)(2,1)} %gate_hbm.1, bf16[1,2048,512]{2,1,0:T(8,128)(2,1)} %up_hbm.1, ...), custom_call_target="tpu_custom_call" | custom-call | tf_op jit(solution)/shard_map/experts/pallas_call | solution.py:466
  106.5 1.9 %copy.37 = bf16[128,2048]{1,0:T(8,128)(2,1)} copy(bf16[128,2048]{1,0:T(8,128)(2,1)} %experts.1) | data formatting | bytes 1048576
  (12 shorter events, 0.2 us)
Async XLA Ops:
  0.0 28.2 %copy-start = (bf16[1024,1024]{1,0:T(8,128)(2,1)S(1)}, bf16[1024,1024]{1,0:T(8,128)(2,1)}, u32[]{:S(2)}) copy-start(bf16[1024,1024]{1,0:T(8,128)(2,1)} %param.23) | copy-start | bytes 6291460
  0.0 6.0 %copy-start.2 = (f32[32,128,16]{1,2,0:T(8,128)S(1)}, f32[32,128,16]{1,2,0:T(8,128)}, u32[]{:S(2)}) copy-start(f32[32,128,16]{1,2,0:T(8,128)} %param.21) | copy-start | bytes 786436
  28.2 3.8 %copy-start.3 = (s32[128,2]{0,1:T(2,128)S(1)}, s32[128,2]{0,1:T(2,128)}, u32[]{:S(2)}) copy-start(s32[128,2]{0,1:T(2,128)} %param.27) | copy-start | bytes 3076
  28.2 4.0 %copy-start.4 = (f32[2048]{0:T(1024)S(1)}, f32[2048]{0:T(1024)}, u32[]{:S(2)}) copy-start(f32[2048]{0:T(1024)} %param.26) | copy-start | bytes 24580
  31.9 3.7 %copy-start.1 = (f32[128,2048]{1,0:T(8,128)}, f32[128,2048]{1,0:T(8,128)S(1)}, u32[]{:S(2)}) copy-start(f32[128,2048]{1,0:T(8,128)S(1)} %get-tuple-element.16.mixed_ref) | copy-start | bytes 3145732
  31.9 1.9 %copy-start.5 = (f32[128,2]{0,1:T(2,128)S(1)}, f32[128,2]{0,1:T(2,128)}, u32[]{:S(2)}) copy-start(f32[128,2]{0,1:T(2,128)} %param.28) | copy-start | bytes 3076
  31.9 2.2 %copy-start.6 = (f32[4]{0:T(128)S(1)}, f32[4]{0:T(128)}, u32[]{:S(2)}) copy-start(f32[4]{0:T(128)} %constant.51) | copy-start | bytes 52
